TPU v7x, 512 devices: a whole 4x8x8 slice. The times are simulated.
512 devices in a mesh: gr: 2 (over z_hi), fs: 32 (over z_lo, y), tp: 8 (over x, core).
Axes of the slice: x: 4, y: 8, z: 8 (z_hi: 2, z_lo: 4; z = z_hi * 4 + z_lo), core: 2. Of those that a mesh axis runs over, the one named last changes fastest.
Arguments:
- tokens: bfloat16 [16384, 2048], P(('gr', 'fs')), may hold values from -6 to 6
- norm_gain: float32 [2048], P(('gr', 'fs')), may hold values from 0.1 to 1.9
- gate_train: float32 [32, 2048, 1024], P(None, ('gr', 'fs'), 'tp'), may hold values from -0.125 to 0.125
- up_train: float32 [32, 2048, 1024], P(None, ('gr', 'fs'), 'tp'), may hold values from -0.125 to 0.125
- down_train: float32 [32, 1024, 2048], P(None, 'tp', ('gr', 'fs')), may hold values from -0.1875 to 0.1875
- expert_ids: int32 [16384, 2], P(('gr', 'fs')), may hold values from 0 to 31, all different within a row; in each aligned block of 256 rows (0 to 255, 256 to 511, ...) at most 32 rows name the same one
- route_score: float32 [16384, 2], P(('gr', 'fs')), may hold values from 0.05 to 1
Outputs:
- gate_ready: bfloat16 [32, 2048, 1024], P('fs', None, 'tp')
- up_ready: bfloat16 [32, 2048, 1024], P('fs', None, 'tp')
- down_ready: bfloat16 [32, 1024, 2048], P('fs', 'tp')
- mixed: bfloat16 [16384, 2048], P(('gr', 'fs'), 'tp')
Inputs may be any that keep to these rules, and one draw needn't show every extreme that they name: `expert_ids`: each row names two different experts. Among the 256 rows of one device no expert is named more than 32 times, and in every draw some expert is named exactly 32 times by some device's rows.
All inputs are finite; a program needn't handle non-finite values.
Results may differ from a plain program's by a relative error of at most 0.015.
Values may be sent and summed in bfloat16 or wider, within the bound.
A program may use at most 64 MiB of HBM per device.

v0:
```python
import jax
import jax.numpy as jnp
from jax import lax
from jax.sharding import PartitionSpec as P

epsilon = 1e-06


def sent_together(arrays, axis, split_dim, concat_dim, along):
    both = jnp.concatenate(arrays, axis=along)
    out, at, outs = (
        lax.all_to_all(both, axis, split_axis=split_dim, concat_axis=concat_dim, tiled=True),
        0,
        [],
    )
    for a in arrays:
        outs.append(lax.slice_in_dim(out, at, at + a.shape[along], axis=along))
        at += a.shape[along]
    return tuple(outs)


def shortened(shard):
    return jax.tree.map(lambda a: a.astype(jnp.bfloat16) if a.dtype == jnp.float32 else a, shard)


def in_order(tiles, dim):
    tiles = jnp.moveaxis(tiles, 0, dim)
    lengths = tiles.shape
    return tiles.reshape(*lengths[:dim], lengths[dim] * lengths[dim + 1], *lengths[dim + 2 :])


def copy_for_each(shard, axis):
    copies = jnp.broadcast_to(shard, (lax.axis_size(axis), *shard.shape))
    return lax.all_to_all(copies, axis, split_axis=0, concat_axis=0, tiled=True)


def gathered_copies(shard, axis, dim):
    return in_order(copy_for_each(shard, axis), dim)


def move_inputs(gate_cast, up_cast):
    spread = sent_together((gate_cast[:, None], up_cast[:, None]), "fs", 0, 1, 2)
    flattened = tuple((piece.reshape(piece.shape[0], 1, -1, piece.shape[-1]) for piece in spread))
    owned = jax.tree.map(
        lambda part, own: part.astype(own.dtype),
        jax.tree.map(lambda part: gathered_copies(part, "gr", 1), shortened(flattened)),
        flattened,
    )
    return tuple((piece.reshape(piece.shape[0], -1, piece.shape[-1]) for piece in owned))


def move_down(down_cast):
    spread = lax.all_to_all(down_cast[:, :, None], "fs", split_axis=0, concat_axis=2, tiled=True)
    flattened = spread.reshape(spread.shape[0], spread.shape[1], 1, -1)
    owned = lax.all_gather(flattened, "gr", axis=2, tiled=True)
    return owned.reshape(owned.shape[0], owned.shape[1], -1)


def on_device(tokens, norm_gain, gate_train, up_train, down_train, expert_ids, route_score):
    gate_cast = (norm_gain[None, :, None] * gate_train).astype(jnp.bfloat16)
    up_cast = (norm_gain[None, :, None] * up_train).astype(jnp.bfloat16)
    down_cast = down_train.astype(jnp.bfloat16)
    fs_count = lax.axis_size("fs")
    tp_count = lax.axis_size("tp")
    experts = gate_train.shape[0]
    tok_count = tokens.shape[0]
    width = tokens.shape[1]
    capacity = 4 * tok_count // experts
    gate_ready, up_ready = move_inputs(gate_cast, up_cast)
    down_ready = move_down(down_cast)
    floated = tokens.astype(jnp.float32)
    normed = (
        floated * lax.rsqrt(jnp.mean(floated * floated, axis=-1, keepdims=True) + epsilon)
    ).astype(jnp.bfloat16)
    flat_ids = expert_ids.reshape(-1)
    matches = (flat_ids[:, None] == jnp.arange(experts, dtype=jnp.int32)[None, :]).astype(jnp.int32)
    ranked = jnp.sum((jnp.cumsum(matches, axis=0) - 1) * matches, axis=1)
    slot_index = flat_ids * capacity + ranked
    pick_token = jnp.arange(flat_ids.shape[0], dtype=jnp.int32) // 2
    slot_token = jnp.zeros((experts * capacity,), jnp.int32).at[slot_index].set(pick_token)
    filled = jnp.zeros((experts * capacity,), jnp.bool_).at[slot_index].set(True)
    gathered_rows = jnp.where(filled[:, None], normed[slot_token], jnp.zeros((), jnp.bfloat16))
    outgoing = gathered_rows.reshape(fs_count, experts // fs_count, capacity, width)
    share_width = width // tp_count
    own_share = lax.dynamic_slice_in_dim(
        outgoing, lax.axis_index("tp") * share_width, share_width, 3
    )
    arrived = lax.all_to_all(own_share, "fs", split_axis=0, concat_axis=0, tiled=True)
    received = lax.all_gather(arrived, "tp", axis=3, tiled=True)
    gate_act = jnp.einsum(
        "seck,ekh->sech", received, gate_ready, preferred_element_type=jnp.float32
    )
    up_act = jnp.einsum("seck,ekh->sech", received, up_ready, preferred_element_type=jnp.float32)
    hidden = (jax.nn.silu(gate_act) * up_act).astype(jnp.bfloat16)
    partial_value = jnp.einsum(
        "sech,ehk->seck", hidden, down_ready, preferred_element_type=jnp.float32
    )
    summed = lax.psum_scatter(
        partial_value.astype(jnp.bfloat16), "tp", scatter_dimension=3, tiled=True
    )
    returned = lax.all_to_all(summed, "fs", split_axis=0, concat_axis=0, tiled=True)
    flat_back = returned.reshape(experts * capacity, -1)
    picked = flat_back[slot_index].reshape(tok_count, 2, -1)
    route_share = route_score / jnp.sum(route_score, axis=-1, keepdims=True)
    mixed = jnp.sum(picked.astype(jnp.float32) * route_share[:, :, None], axis=1).astype(
        jnp.bfloat16
    )
    return (gate_ready, up_ready, down_ready, mixed)


def solution(mesh):
    return jax.shard_map(
        on_device,
        mesh=mesh,
        in_specs=(
            P(("gr", "fs"), None),
            P(("gr", "fs")),
            P(None, ("gr", "fs"), "tp"),
            P(None, ("gr", "fs"), "tp"),
            P(None, "tp", ("gr", "fs")),
            P(("gr", "fs"), None),
            P(("gr", "fs"), None),
        ),
        out_specs=(
            P("fs", None, "tp"),
            P("fs", None, "tp"),
            P("fs", "tp", None),
            P(("gr", "fs"), "tp"),
        ),
        check_vma=False,
    )
```

profile of v0, /device:TPU:15, one launch (start us, length us, event | category | flops | bytes accessed | tf_op | source)
XLA Modules:
  0.0 236.6 jit_solution(1337463816797035005)
XLA Ops:
  9.0 1.2 reduce-window.6
  10.9 2.4 %scatter_custom_fusion.1 = s32[1024]{0:T(1024)S(1)} fusion(s32[512]{0:T(512)S(1)} %bitcast.107, s32[512]{0:T(512)S(1)} %add_select_fusion, s32[]{:T(128)} %constant.20.clone.1), kind=kCustom, calls=%fused_computation.50 | custom fusion | bytes 4100 | tf_op jit(solution)/shard_map/scatter | solution.py:80
  13.3 1.5 fusion.4
  14.9 1.5 fusion.5
  16.3 2.4 %scatter_custom_fusion = pred[1024]{0:T(1024)(128)(4,1)S(1)} fusion(s32[512]{0:T(512)S(1)} %bitcast.108, pred[512]{0:T(512)(128)(4,1)S(1)} %broadcast.106, pred[]{:T(512)} %constant.17.clone.1), kind=kCustom, calls=%fused_computation.53 | custom fusion | bytes 1025 | tf_op jit(solution)/shard_map/scatter | solution.py:81
  18.9 6.0 %gather_fusion = bf16[1024,2048]{1,0:T(8,128)(2,1)} fusion(bf16[256,2048]{1,0:T(8,128)(2,1)S(1)} %fusion.5, s32[1024]{0:T(1024)S(1)} %fusion.34), kind=kCustom, calls=%fused_computation | custom fusion | bytes 8392704 | tf_op jit(solution)/shard_map/gather | solution.py:82
  24.9 1.3 dynamic-slice_select_fusion
  26.2 28.4 %all_to_all.47 = bf16[32,1,32,256]{3,2,1,0:T(8,128)(2,1)} all-to-all(bf16[32,1,32,256]{3,2,1,0:T(8,128)(2,1)S(1)} %dynamic-slice_select_fusion), channel_id=1, replica_groups=mesh['gr'=2,'fs'=32,'tp'=8] {'fs'}, dimensions={0} | all-to-all | bytes 1048576 | tf_op jit(solution)/shard_map/all_to_all | solution.py:88
  55.7 6.0 %all-to-all-start = ((bf16[32,1,64,128]{3,2,1,0:T(8,128)(2,1)}), bf16[32,1,64,128]{3,2,1,0:T(8,128)(2,1)S(1)}, u32[]{:S(2)}, u32[]{:S(2)}) async-start(bf16[32,1,64,128]{3,2,1,0:T(8,128)(2,1)} %pad_maximum_fusion), calls=%async_computation | async-start | bytes 1048576 | tf_op jit(solution)/shard_map/all_to_all | solution.py:12
  62.5 15.0 %all-to-all-done = bf16[32,1,64,128]{3,2,1,0:T(8,128)(2,1)S(1)} async-done(((bf16[32,1,64,128]{3,2,1,0:T(8,128)(2,1)}), bf16[32,1,64,128]{3,2,1,0:T(8,128)(2,1)S(1)}, u32[]{:S(2)}, u32[]{:S(2)}) %all-to-all-start) | async-done | bytes 524320 | tf_op jit(solution)/shard_map/all_to_all | solution.py:12
  77.5 6.2 %all-to-all-start.3 = ((bf16[32,128,1,32]{1,3,2,0:T(8,128)(2,1)}), bf16[32,128,1,32]{1,3,2,0:T(8,128)(2,1)S(1)}, u32[]{:S(2)}, u32[]{:S(2)}) async-start(bf16[32,128,1,32]{1,3,2,0:T(8,128)(2,1)} %convert_bitcast_fusion.1), calls=%async_computation.3 | async-start | bytes 524288 | tf_op jit(solution)/shard_map/all_to_all | solution.py:53
  83.7 10.8 %all-to-all-done.3 = bf16[32,128,1,32]{1,3,2,0:T(8,128)(2,1)S(1)} async-done(((bf16[32,128,1,32]{1,3,2,0:T(8,128)(2,1)}), bf16[32,128,1,32]{1,3,2,0:T(8,128)(2,1)S(1)}, u32[]{:S(2)}, u32[]{:S(2)}) %all-to-all-start.3) | async-done | bytes 262176 | tf_op jit(solution)/shard_map/all_to_all | solution.py:53
  95.3 7.3 %all-to-all-start.1 = ((bf16[2,1,1,1024,128]{4,3,2,1,0:T(8,128)(2,1)}), bf16[2,1,1,1024,128]{4,3,2,1,0:T(8,128)(2,1)S(1)}, u32[]{:S(2)}, u32[]{:S(2)}) async-start(bf16[2,1,1,1024,128]{4,3,2,1,0:T(8,128)(2,1)} %broadcast_in_dim.50), calls=%async_computation.1 | async-start | bytes 1048576 | tf_op jit(solution)/shard_map/all_to_all | solution.py:34
  102.8 9.5 %all-to-all-done.1 = bf16[2,1,1,1024,128]{4,3,2,1,0:T(8,128)(2,1)S(1)} async-done(((bf16[2,1,1,1024,128]{4,3,2,1,0:T(8,128)(2,1)}), bf16[2,1,1,1024,128]{4,3,2,1,0:T(8,128)(2,1)S(1)}, u32[]{:S(2)}, u32[]{:S(2)}) %all-to-all-start.1) | async-done | bytes 524320 | tf_op jit(solution)/shard_map/all_to_all | solution.py:34
  113.1 3.5 %all-to-all-start.2 = ((bf16[2,1,1,1024,128]{4,3,2,1,0:T(8,128)(2,1)}), bf16[2,1,1,1024,128]{4,3,2,1,0:T(8,128)(2,1)S(1)}, u32[]{:S(2)}, u32[]{:S(2)}) async-start(bf16[2,1,1,1024,128]{4,3,2,1,0:T(8,128)(2,1)} %broadcast_in_dim.51), calls=%async_computation.2 | async-start | bytes 1048576 | tf_op jit(solution)/shard_map/all_to_all | solution.py:34
  116.7 12.1 %all_gather.6 = bf16[1,128,2,1024]{3,1,0,2:T(8,128)(2,1)S(1)} all-gather(bf16[1,128,1,1024]{3,1,0,2:T(8,128)(2,1)S(1)} %copy.31), channel_id=1, replica_groups=mesh['gr'=2,'fs'=32,'tp'=8] {'gr'}, dimensions={2}, use_global_device_ids=true | all-gather | bytes 786432 | tf_op jit(solution)/shard_map/all_gather | solution.py:55
  129.7 3.4 %fusion.6 = f32[32,1,32,128]{3,2,0,1:T(8,128)S(1)} fusion(bf16[2048,128,1]{1,0,2:T(8,128)(2,1)S(1)} %bitcast.98, bf16[32,1,32,2048]{3,2,0,1:T(8,128)(2,1)} %all-gather.2.cloned.1.call-done), kind=kOutput, calls=%fused_computation.13 | convolution fusion | flops 536870912 | bytes 5242880 | tf_op jit(solution)/shard_map/seck,ekh->sech/dot_general | solution.py:90
  133.2 8.5 %convert_bitcast_fusion = bf16[32,1,32,2048]{3,2,0,1:T(8,128)(2,1)} fusion(bf16[128,2048,1]{1,0,2:T(8,128)(2,1)S(1)} %reshape.182, bf16[2048,128,1]{1,0,2:T(8,128)(2,1)S(1)} %bitcast.96, bf16[32,1,32,2048]{3,2,0,1:T(8,128)(2,1)} %all-gather.2.cloned.1.call-done, f32[32,1,32,128]{3,2,0,1:T(8,128)S(1)} %fusion.6), kind=kOutput, calls=%fused_computation.8 | convolution fusion | flops 1076625408 | bytes 9961472 | tf_op jit(solution)/shard_map/sech,ehk->seck/dot_general | solution.py:95
  141.7 55.0 %reduce-scatter.2.cloned.1.call-done = bf16[32,1,32,256]{3,2,0,1:T(8,128)(2,1)} async-done(((bf16[32,1,32,2048]{3,2,0,1:T(8,128)(2,1)}), bf16[32,1,32,256]{3,2,0,1:T(8,128)(2,1)}) %reduce-scatter.2.cloned.1.call-update) | async-done | bytes 524304 | tf_op jit(solution)/shard_map/reduce_scatter | solution.py:98
  196.7 10.2 %all-to-all-start.5 = ((bf16[32,1,32,256]{3,2,1,0:T(8,128)(2,1)}), bf16[32,1,32,256]{3,2,1,0:T(8,128)(2,1)S(1)}, u32[]{:S(2)}, u32[]{:S(2)}) async-start(bf16[32,1,32,256]{3,2,1,0:T(8,128)(2,1)} %bitcast.106), calls=%async_computation.6 | async-start | bytes 1048576 | tf_op jit(solution)/shard_map/all_to_all | solution.py:101
  207.4 1.0 copy.42
  208.4 16.1 %all-to-all-done.5 = bf16[32,1,32,256]{3,2,1,0:T(8,128)(2,1)S(1)} async-done(((bf16[32,1,32,256]{3,2,1,0:T(8,128)(2,1)}), bf16[32,1,32,256]{3,2,1,0:T(8,128)(2,1)S(1)}, u32[]{:S(2)}, u32[]{:S(2)}) %all-to-all-start.5) | async-done | bytes 524320 | tf_op jit(solution)/shard_map/all_to_all | solution.py:101
  224.5 1.9 gather_fusion.1
  226.8 1.4 multiply_reduce_fusion
  (50 shorter events, 9.5 us)
Async XLA Ops:
  7.2 122.5 %all-gather.2.cloned.1.call-start = ((), (), s32[]{:S(2)}) async-start(), calls=%async_computation.7 | async-start | bytes 4718592 | tf_op jit(solution)/shard_map/all_gather | solution.py:89
  18.9 35.8 %copy-start.1 = (f32[32,32,128]{2,1,0:T(8,128)S(1)}, f32[32,32,128]{2,1,0:T(8,128)}, u32[]{:S(2)}) copy-start(f32[32,32,128]{2,1,0:T(8,128)} %param.9) | copy-start | bytes 1572868
  18.9 35.8 %copy-start.2 = (f32[32,32,128]{2,1,0:T(8,128)S(1)}, f32[32,32,128]{2,1,0:T(8,128)}, u32[]{:S(2)}) copy-start(f32[32,32,128]{2,1,0:T(8,128)} %param.10) | copy-start | bytes 1572868
  18.9 35.8 %copy-start.4 = (f32[32]{0:T(128)S(1)}, f32[32]{0:T(128)}, u32[]{:S(2)}) copy-start(f32[32]{0:T(128)} %param.8) | copy-start | bytes 388
  24.9 36.8 %copy-start = (f32[32,128,32]{1,2,0:T(8,128)S(1)}, f32[32,128,32]{1,2,0:T(8,128)}, u32[]{:S(2)}) copy-start(f32[32,128,32]{1,2,0:T(8,128)} %param.11) | copy-start | bytes 1572868
  55.7 21.8 %all-to-all-start = ((bf16[32,1,64,128]{3,2,1,0:T(8,128)(2,1)}), bf16[32,1,64,128]{3,2,1,0:T(8,128)(2,1)S(1)}, u32[]{:S(2)}, u32[]{:S(2)}) async-start(bf16[32,1,64,128]{3,2,1,0:T(8,128)(2,1)} %pad_maximum_fusion), calls=%async_computation | async-start | bytes 1048576 | tf_op jit(solution)/shard_map/all_to_all | solution.py:12
  77.5 17.0 %all-to-all-start.3 = ((bf16[32,128,1,32]{1,3,2,0:T(8,128)(2,1)}), bf16[32,128,1,32]{1,3,2,0:T(8,128)(2,1)S(1)}, u32[]{:S(2)}, u32[]{:S(2)}) async-start(bf16[32,128,1,32]{1,3,2,0:T(8,128)(2,1)} %convert_bitcast_fusion.1), calls=%async_computation.3 | async-start | bytes 524288 | tf_op jit(solution)/shard_map/all_to_all | solution.py:53
  95.3 17.0 %all-to-all-start.1 = ((bf16[2,1,1,1024,128]{4,3,2,1,0:T(8,128)(2,1)}), bf16[2,1,1,1024,128]{4,3,2,1,0:T(8,128)(2,1)S(1)}, u32[]{:S(2)}, u32[]{:S(2)}) async-start(bf16[2,1,1,1024,128]{4,3,2,1,0:T(8,128)(2,1)} %broadcast_in_dim.50), calls=%async_computation.1 | async-start | bytes 1048576 | tf_op jit(solution)/shard_map/all_to_all | solution.py:34
  113.1 20.0 %all-to-all-start.2 = ((bf16[2,1,1,1024,128]{4,3,2,1,0:T(8,128)(2,1)}), bf16[2,1,1,1024,128]{4,3,2,1,0:T(8,128)(2,1)S(1)}, u32[]{:S(2)}, u32[]{:S(2)}) async-start(bf16[2,1,1,1024,128]{4,3,2,1,0:T(8,128)(2,1)} %broadcast_in_dim.51), calls=%async_computation.2 | async-start | bytes 1048576 | tf_op jit(solution)/shard_map/all_to_all | solution.py:34
  116.6 80.1 %reduce-scatter.2.cloned.1.call-start = ((), (), s32[]{:S(2)}) async-start(), calls=%async_computation.8 | async-start | bytes 4718592 | tf_op jit(solution)/shard_map/reduce_scatter | solution.py:98
  141.7 65.3 %copy-start.3 = (f32[256,2]{0,1:T(2,128)S(1)}, f32[256,2]{0,1:T(2,128)}, u32[]{:S(2)}) copy-start(f32[256,2]{0,1:T(2,128)} %param.13) | copy-start | bytes 6148
  196.7 27.8 %all-to-all-start.5 = ((bf16[32,1,32,256]{3,2,1,0:T(8,128)(2,1)}), bf16[32,1,32,256]{3,2,1,0:T(8,128)(2,1)S(1)}, u32[]{:S(2)}, u32[]{:S(2)}) async-start(bf16[32,1,32,256]{3,2,1,0:T(8,128)(2,1)} %bitcast.106), calls=%async_computation.6 | async-start | bytes 1048576 | tf_op jit(solution)/shard_map/all_to_all | solution.py:101
Sparse Core Ops, SparseCore 0:
  54.8 40.9 all-gather.1
  141.8 54.8 reduce-scatter.1
where the time goes:
time: 237 us
  waiting for transfers between devices  107 us (45%)
  blocking collectives  40.5 us (17%)
  starting transfers between devices  33.2 us (14%)
  local copies, waits for them, and re-layouts  20.6 us (9%)
  between operations  14.3 us (6%)
  matrix products  11.9 us (5%)
  other arithmetic  9.49 us (4%)
    reduce_scatter x1, waiting for transfers between devices, on_device(): lax.psum_scatter(partial_value.astype(jnp.bfloat16), 'tp', scatter_dimens...  55 us
    all_to_all x1, blocking collectives, on_device(): lax.all_to_all(own_share, 'fs', split_axis=0, concat_axis=0, tiled=True)  28.4 us
    all_to_all x1, waiting for transfers between devices, on_device(): lax.all_to_all(summed, 'fs', split_axis=0, concat_axis=0, tiled=True)  16.1 us
    all_to_all x1, waiting for transfers between devices, sent_together(): lax.all_to_all(both, axis, split_axis=split_dim, concat_axis=concat_dim,...  15 us
    all_gather x1, blocking collectives, move_down(): owned = lax.all_gather(flattened, 'gr', axis=2, tiled=True)  12.1 us
    all_to_all x2, starting transfers between devices, copy_for_each(): return lax.all_to_all(copies, axis, split_axis=0, concat_axis=0, tiled=True)  10.8 us
    all_to_all x1, waiting for transfers between devices, move_down(): lax.all_to_all(down_cast[:, :, None], 'fs', split_axis=0, concat_axis=2,...  10.8 us
    all_to_all x1, starting transfers between devices, on_device(): lax.all_to_all(summed, 'fs', split_axis=0, concat_axis=0, tiled=True)  10.2 us
  transfers between devices with their start and end apart: 7, of which 5 were waited for; matrix products, arithmetic and copies ran while one was open for 4% of the time, Pallas kernels for 0%

commit v1 on v0

v1 whole, which is shorter than its diff:
```python
import jax
import jax.numpy as jnp
from jax import lax
from jax.experimental import pallas as pl
from jax.experimental.pallas import tpu as pltpu
from jax.sharding import PartitionSpec as P

EPS = 1e-06
NY, NZ, NX = 8, 4, 4
NF = NY * NZ
CAP = 32
MESH = pl.DeviceIdType.MESH
BF, F32 = jnp.bfloat16, jnp.float32


def ring_offset(j, n):
    return jnp.where(j % 2 == 1, (j + 1) // 2, n - j // 2)


def kernel(
    tok, ids_t, score, gain, gate, up, down,
    gate_o, up_o, down_o, mixed_o,
    wsend, wy, wz, tsend, xin, rt, p0, p1, own, psend, precv, sbuf, r1, r2, fin, ret,
    wy_r, wz_r, tk_r, g_r, s_r, ret_r, snd,
):
    g, f, t = lax.axis_index("gr"), lax.axis_index("fs"), lax.axis_index("tp")
    z, y, x, c = f // NY, f % NY, t // 2, t % 2
    zz = g * NZ + z
    right, left = ((x + 1) % NX) * 2 + c, ((x + 3) % NX) * 2 + c
    opp, part = ((x + 2) % NX) * 2 + c, x * 2 + (1 - c)

    def send(src, dst, ssem, rsem, dev):
        pltpu.make_async_remote_copy(
            src_ref=src, dst_ref=dst, send_sem=ssem, recv_sem=rsem,
            device_id=dev, device_id_type=MESH,
        ).start()

    def arrived(dst, rsem):
        pltpu.make_async_remote_copy(
            src_ref=dst, dst_ref=dst, send_sem=snd.at[0], recv_sem=rsem,
            device_id=(g, f, part), device_id_type=MESH,
        ).wait_recv()

    def sent(ref, ssem):
        pltpu.make_async_remote_copy(
            src_ref=ref, dst_ref=ref, send_sem=ssem, recv_sem=wy_r.at[0],
            device_id=(g, f, part), device_id_type=MESH,
        ).wait_send()

    def loop(lo, hi, fn):
        def body(i, carry):
            fn(i)
            return carry
        lax.fori_loop(lo, hi, body, 0)

    bar = pltpu.get_barrier_semaphore()

    def greet(dev):
        pl.semaphore_signal(bar, inc=1, device_id=dev, device_id_type=MESH)

    loop(1, NF, lambda i: greet((g, (f + i) % NF, t)))
    loop(0, NZ, lambda i: greet((1 - g, i * NY + y, t)))
    for tt in (right, left, part):
        greet((g, f, tt))

    def cast(e):
        yy, z2 = e % NY, e // NY
        wsend[yy, z2, 0:32, :] = (gain[...] * gate[e]).astype(BF)
        wsend[yy, z2, 32:64, :] = (gain[...] * up[e]).astype(BF)
        wsend[yy, z2, 64:96, :] = down[e].T.astype(BF)

    loop(0, NF, cast)
    pl.semaphore_wait(bar, NF - 1 + NZ + 3)

    def y_send(j):
        yy = (y + ring_offset(j, NY)) % NY
        send(wsend.at[yy], wy.at[y], snd.at[0], wy_r.at[y], (g, z * NY + yy, t))

    def z_send(block, s):
        row = zz * NY + s

        def one(j):
            to = (zz + ring_offset(j, 2 * NZ)) % (2 * NZ)
            send(block.at[to % NZ], wz.at[row], snd.at[1], wz_r.at[row],
                 (to // NZ, (to % NZ) * NY + y, t))

        loop(1, 2 * NZ, one)
        wz[row] = block[z]

    loop(1, NY, y_send)
    z_send(wsend.at[y], y)

    e_iota = lax.broadcasted_iota(jnp.int32, (NF, 256), 0)
    i0, i1 = ids_t[0:1, :], ids_t[1:2, :]
    hit = (i0 == e_iota) | (i1 == e_iota)
    before = (
        lax.broadcasted_iota(jnp.int32, (256, 256), 0)
        < lax.broadcasted_iota(jnp.int32, (256, 256), 1)
    )
    rank = jnp.dot(hit.astype(F32).astype(BF), before.astype(F32).astype(BF),
                   preferred_element_type=F32)
    rt[...] = jnp.where(hit, rank, -1.0)
    r_iota = lax.broadcasted_iota(jnp.int32, (CAP, 256), 0).astype(F32)

    def slots(e):
        mask = rt[pl.ds(e, 1), :] == r_iota
        p0[e] = jnp.where(mask & (ids_t[0:1, :] == e), 1.0, 0.0).astype(BF)
        p1[e] = jnp.where(mask & (ids_t[1:2, :] == e), 1.0, 0.0).astype(BF)

    loop(0, NF, slots)
    floated = tok[...].astype(F32)
    inv = lax.rsqrt(jnp.mean(floated * floated, axis=-1, keepdims=True) + EPS)
    cols = pl.ds(pl.multiple_of(t * 256, 256), 256)
    normed = (tok[:, cols].astype(F32) * inv).astype(BF)

    def gather_rows(b):
        e = pl.ds(b * 8, 8)
        pick = (p0[e] + p1[e]).reshape(256, 256)
        rows = jnp.dot(pick, normed, preferred_element_type=F32)
        tsend[e] = rows.astype(BF).reshape(8, CAP, 256)

    loop(0, NZ, gather_rows)

    def t_send(i):
        zt = (z + i // NY) % NZ
        e = zt * NY + (y + i % NY) % NY
        send(tsend.at[e], xin.at[t, f], snd.at[2], tk_r.at[f], (g, e, t))

    loop(1, NF, t_send)
    xin[t, f] = tsend[f]

    def y_forward(j):
        s = (y + NY - ring_offset(j, NY)) % NY
        arrived(wy.at[s], wy_r.at[s])
        z_send(wy.at[s], s)

    loop(1, NY, y_forward)

    def chunk(k):
        return (z + NZ - k) % NZ

    def x_first(k):
        q = chunk(k)

        def one(i):
            s = q * NY + i

            @pl.when(s != f)
            def _():
                arrived(xin.at[t, s], tk_r.at[s])

        loop(0, NY, one)
        blk = xin.at[t, pl.ds(q * NY, NY)]
        send(blk, blk, snd.at[3], g_r.at[0, k], (g, f, right))
        send(blk, blk, snd.at[3], g_r.at[1, k], (g, f, left))
        send(blk, blk, snd.at[3], g_r.at[4, k], (g, f, part))

    def x_second(k):
        q = chunk(k)
        for side, kind, to, lo in ((left, 0, right, 0), (right, 1, left, 4)):
            blk = xin.at[side, pl.ds(q * NY, NY)]
            half = xin.at[side, pl.ds(q * NY + lo, 4)]
            arrived(blk, g_r.at[kind, k])
            send(half, half, snd.at[3], g_r.at[kind + 2, k], (g, f, to))
            send(blk, blk, snd.at[3], g_r.at[kind + 5, k], (g, f, part))

    def x_third(k):
        q = chunk(k)
        arrived(xin.at[opp, pl.ds(q * NY, 4)], g_r.at[2, k])
        arrived(xin.at[opp, pl.ds(q * NY + 4, 4)], g_r.at[3, k])
        blk = xin.at[opp, pl.ds(q * NY, NY)]
        send(blk, blk, snd.at[3], g_r.at[7, k], (g, f, part))

    def x_step(k):
        @pl.when(k < NZ)
        def _():
            x_first(k)

        @pl.when((k >= 1) & (k < NZ + 1))
        def _():
            x_second(k - 1)

        @pl.when(k >= 2)
        def _():
            x_third(k - 2)

    loop(0, NZ + 2, x_step)
    flip = 1 - 2 * c

    def from_partner(k):
        q = pl.ds(chunk(k) * NY, NY)
        for side, kind in ((part, 4), (left + flip, 5), (right + flip, 6), (opp + flip, 7)):
            arrived(xin.at[side, q], g_r.at[kind, k])

    loop(0, NZ, from_partner)

    def w_arrived(i):
        @pl.when(i // NY != zz)
        def _():
            arrived(wz.at[i], wz_r.at[i])

    loop(0, 2 * NF, w_arrived)

    def layer(k):
        q = pl.ds(chunk(k) * NY, NY)
        acc = jnp.zeros((256, 256), F32)
        for s in range(8):
            w = jnp.concatenate(
                [wz[8 * s:8 * s + 8, 0:32, :].reshape(256, 128),
                 wz[8 * s:8 * s + 8, 32:64, :].reshape(256, 128)], axis=1)
            acc += jnp.dot(xin[s, q].reshape(256, 256), w, preferred_element_type=F32)
        a, b = acc[:, 0:128], acc[:, 128:256]
        hidden = (a / (1.0 + jnp.exp(-a)) * b).astype(BF)
        for j in range(NX):
            for cc in (1 - c, c):
                blk = ((x + j) % NX) * 2 + cc
                d = wz[pl.ds(blk * 8, 8), 64:96, :].reshape(256, 128)
                o = lax.dot_general(hidden, d, (((1,), (1,)), ((), ())),
                                    preferred_element_type=F32)
                if cc is c:
                    own[k, j] = o
                else:
                    psend[k, j] = o.astype(BF)
        send(psend.at[k], precv.at[k], snd.at[4], s_r.at[0, k], (g, f, part))

    def r_first(k):
        arrived(precv.at[k], s_r.at[0, k])
        sbuf[k, 1] = (own[k, 2] + precv[k, 2].astype(F32)).astype(BF)
        send(sbuf.at[k, 1, pl.ds(0, 128)], r1.at[k, 0], snd.at[5], s_r.at[1, k], (g, f, right))
        send(sbuf.at[k, 1, pl.ds(128, 128)], r1.at[k, 1], snd.at[5], s_r.at[2, k], (g, f, left))

    def r_second(k):
        lo, hi = pl.ds(0, 128), pl.ds(128, 128)
        arrived(r1.at[k, 0], s_r.at[1, k])
        sbuf[k, 0, lo] = (own[k, 1, lo] + precv[k, 1, lo].astype(F32) + r1[k, 0].astype(F32)).astype(BF)
        sbuf[k, 0, hi] = (own[k, 1, hi] + precv[k, 1, hi].astype(F32)).astype(BF)
        send(sbuf.at[k, 0], r2.at[k, 0], snd.at[6], s_r.at[3, k], (g, f, right))
        arrived(r1.at[k, 1], s_r.at[2, k])
        sbuf[k, 2, lo] = (own[k, 3, lo] + precv[k, 3, lo].astype(F32)).astype(BF)
        sbuf[k, 2, hi] = (own[k, 3, hi] + precv[k, 3, hi].astype(F32) + r1[k, 1].astype(F32)).astype(BF)
        send(sbuf.at[k, 2], r2.at[k, 1], snd.at[6], s_r.at[4, k], (g, f, left))

    def r_third(k):
        arrived(r2.at[k, 0], s_r.at[3, k])
        arrived(r2.at[k, 1], s_r.at[4, k])
        total = (own[k, 0] + precv[k, 0].astype(F32)) + r2[k, 0].astype(F32) + r2[k, 1].astype(F32)
        q = chunk(k)
        fin[q] = total.astype(BF).reshape(NY, CAP, 256)

        def back(i):
            s = q * NY + i

            @pl.when(s != f)
            def _():
                send(fin.at[q, i], ret.at[f], snd.at[7], ret_r.at[f], (g, s, t))

            @pl.when(s == f)
            def _():
                ret[s] = fin[q, i]

        loop(0, NY, back)

    def r_step(k):
        @pl.when(k < NZ)
        def _():
            layer(k)

        @pl.when((k >= 1) & (k < NZ + 1))
        def _():
            r_first(k - 1)

        @pl.when((k >= 2) & (k < NZ + 2))
        def _():
            r_second(k - 2)

        @pl.when(k >= 3)
        def _():
            r_third(k - 3)

    loop(0, NZ + 3, r_step)

    def store(i):
        rows = pl.ds(pl.multiple_of(i * 32, 32), 32)
        gate_o[0, rows, :] = wz[i, 0:32, :]
        up_o[0, rows, :] = wz[i, 32:64, :]

    loop(0, 2 * NF, store)
    for j in range(16):
        blk = wz[4 * j:4 * j + 4, 64:96, :].reshape(128, 128)
        down_o[0, :, 128 * j:128 * j + 128] = blk.astype(F32).T.astype(BF)

    def back_arrived(i):
        @pl.when(i != f)
        def _():
            arrived(ret.at[i], ret_r.at[i])

    loop(0, NF, back_arrived)
    rows = ret[...].reshape(NF * CAP, 256)
    dims = (((0,), (0,)), ((), ()))
    a = lax.dot_general(p0[...].reshape(NF * CAP, 256), rows, dims, preferred_element_type=F32)
    b = lax.dot_general(p1[...].reshape(NF * CAP, 256), rows, dims, preferred_element_type=F32)
    s0, s1 = score[:, 0:1], score[:, 1:2]
    both = s0 + s1
    mixed_o[...] = (a * (s0 / both) + b * (s1 / both)).astype(BF)

    sent(wsend.at[pl.ds(0, 7)], snd.at[0])
    sent(wz.at[pl.ds(0, 56)], snd.at[1])
    sent(tsend.at[pl.ds(0, NF - 1)], snd.at[2])
    sent(xin.at[pl.ds(0, 7)], snd.at[3])
    sent(psend, snd.at[4])
    sent(r1, snd.at[5])
    sent(r2, snd.at[6])
    sent(ret.at[pl.ds(0, NF - 1)], snd.at[7])


def on_device(tokens, norm_gain, gate_train, up_train, down_train, expert_ids, route_score):
    vm = pl.BlockSpec(memory_space=pltpu.VMEM)
    dma = pltpu.SemaphoreType.DMA
    sds = jax.ShapeDtypeStruct
    return tuple(pl.pallas_call(
        kernel,
        out_shape=(
            sds((1, 2048, 128), BF), sds((1, 2048, 128), BF), sds((1, 128, 2048), BF),
            sds((256, 256), BF),
        ),
        in_specs=[vm] * 7,
        out_specs=(vm,) * 4,
        scratch_shapes=[
            pltpu.VMEM((NY, NZ, 96, 128), BF),
            pltpu.VMEM((NY, NZ, 96, 128), BF),
            pltpu.VMEM((2 * NF, 96, 128), BF),
            pltpu.VMEM((NF, CAP, 256), BF),
            pltpu.VMEM((8, NF, CAP, 256), BF),
            pltpu.VMEM((NF, 256), F32),
            pltpu.VMEM((NF, CAP, 256), BF),
            pltpu.VMEM((NF, CAP, 256), BF),
            pltpu.VMEM((NZ, NX, 256, 256), F32),
            pltpu.VMEM((NZ, NX, 256, 256), BF),
            pltpu.VMEM((NZ, NX, 256, 256), BF),
            pltpu.VMEM((NZ, 3, 256, 256), BF),
            pltpu.VMEM((NZ, 2, 128, 256), BF),
            pltpu.VMEM((NZ, 2, 256, 256), BF),
            pltpu.VMEM((NZ, NY, CAP, 256), BF),
            pltpu.VMEM((NF, CAP, 256), BF),
            dma((NY,)), dma((2 * NF,)), dma((NF,)), dma((8, NZ)), dma((5, NZ)), dma((NF,)), dma((8,)),
        ],
        compiler_params=pltpu.CompilerParams(collective_id=0, has_side_effects=True),
    )(
        tokens, expert_ids.T, route_score, norm_gain[:, None], gate_train, up_train, down_train
    ))


def solution(mesh):
    return jax.shard_map(
        on_device,
        mesh=mesh,
        in_specs=(
            P(("gr", "fs"), None),
            P(("gr", "fs")),
            P(None, ("gr", "fs"), "tp"),
            P(None, ("gr", "fs"), "tp"),
            P(None, "tp", ("gr", "fs")),
            P(("gr", "fs"), None),
            P(("gr", "fs"), None),
        ),
        out_specs=(
            P("fs", None, "tp"),
            P("fs", None, "tp"),
            P("fs", "tp", None),
            P(("gr", "fs"), "tp"),
        ),
        check_vma=False,
    )
```

time: 237 us -> 111 us (0.47)
  the two profiles are of different devices: /device:TPU:15 before, /device:TPU:1 now
where the time goes in v1:
time: 111 us; the launch traced here: 110 us
  Pallas kernels  98.8 us (89%)
  local copies, waits for them, and re-layouts  11.1 us (10%)
    pallas_call x1, Pallas kernels, on_device(): pl.pallas_call(kernel, out_shape=(sds((1, 2048, 128), BF), sds((1, 2048,...  98.8 us
    unnamed x10, local copies, waits for them, and re-layouts  9.72 us

profile of v1, /device:TPU:1, one launch (start us, length us, event | category | flops | bytes accessed | tf_op | source)
XLA Modules:
  0.0 110.5 jit_solution(17283171788968497556)
XLA Ops:
  0.6 1.3 %copy.12.gain = f32[32,1]{1,0:T(8,128)} copy(f32[32,1]{0,1:T(1,128)} %bitcast.3) | data formatting | bytes 256 | tf_op jit(solution)/shard_map/broadcast_in_dim | solution.py:349
  2.0 1.5 %copy.11.score = f32[256,2]{1,0:T(8,128)} copy(f32[256,2]{0,1:T(2,128)} %param.13) | data formatting | bytes 4096 | tf_op args[6]
  3.4 3.0 %copy.13.down = f32[32,128,32]{2,1,0:T(8,128)} copy(f32[32,128,32]{1,2,0:T(8,128)} %param.11) | data formatting | bytes 1048576 | tf_op args[4]
  6.4 98.8 %shard_map.102 = (bf16[1,2048,128]{2,1,0:T(8,128)(2,1)}, bf16[1,2048,128]{2,1,0:T(8,128)(2,1)}, bf16[1,128,2048]{2,1,0:T(8,128)(2,1)}, bf16[256,256]{1,0:T(8,128)(2,1)}) custom-call(bf16[256,2048]{1,0:T(8,128)(2,1)} %tok.1, s32[2,256]{1,0:T(2,128)} %bitcast.2, f32[256,2]{1,0:T(8,128)} %copy.11.score, f32[32,1]{1,0:T(8,128)} %copy.12.gain, ...), custom_call_target="tpu_custom_call" | custom-call | tf_op jit(solution)/shard_map/pallas_call | solution.py:320
  105.2 0.0 copy-start
  105.2 0.0 copy-start.1
  105.2 1.9 %copy.18 = bf16[1,2048,128]{2,1,0:T(8,128)(2,1)} copy(bf16[1,2048,128]{2,1,0:T(8,128)(2,1)} %get-tuple-element.8) | data formatting | bytes 1048576
  107.2 1.9 %copy.19 = bf16[1,2048,128]{2,1,0:T(8,128)(2,1)} copy(bf16[1,2048,128]{2,1,0:T(8,128)(2,1)} %get-tuple-element.9) | data formatting | bytes 1048576
  109.0 0.0 copy-done
  109.0 0.8 copy.20
  109.8 0.0 copy-done.1
  109.8 0.7 copy.21
Async XLA Ops:
  105.2 3.8 %copy-start = (bf16[1,128,2048]{2,1,0:T(8,128)(2,1)S(1)}, bf16[1,128,2048]{2,1,0:T(8,128)(2,1)}, u32[]{:S(2)}) copy-start(bf16[1,128,2048]{2,1,0:T(8,128)(2,1)} %get-tuple-element.10) | copy-start | bytes 1572868
  105.2 4.6 %copy-start.1 = (bf16[256,256]{1,0:T(8,128)(2,1)S(1)}, bf16[256,256]{1,0:T(8,128)(2,1)}, u32[]{:S(2)}) copy-start(bf16[256,256]{1,0:T(8,128)(2,1)} %get-tuple-element.11) | copy-start | bytes 393220

commit v2 on v1

v2 whole, which is shorter than its diff:
```python
import jax
import jax.numpy as jnp
from jax import lax
from jax.experimental import pallas as pl
from jax.experimental.pallas import tpu as pltpu
from jax.sharding import PartitionSpec as P

EPS = 1e-06
NY, NZ, NX = 8, 4, 4
NF = NY * NZ
NR = 2 * NZ
CAP = 32
CH, RB = 8, 128
LAG1, LAG2 = 2, 2
MESH = pl.DeviceIdType.MESH
BF, F32 = jnp.bfloat16, jnp.float32


def ring_offset(j, n):
    return jnp.where(j % 2 == 1, (j + 1) // 2, (n - j // 2) % n)


def loop(lo, hi, fn):
    def body(i, carry):
        fn(i)
        return carry

    lax.fori_loop(lo, hi, body, 0)


def column(row, n):
    eye = lax.broadcasted_iota(jnp.int32, (n, n), 0) == lax.broadcasted_iota(jnp.int32, (n, n), 1)
    return jnp.sum(jnp.where(eye, row, 0.0), axis=1, keepdims=True)


def kernel(
    tok, ids_t, score_t, gain_t, gate, up, down_t,
    gate_o, up_o, down_o, mixed_o,
    gain, wg, wd, wyg, wyd, zg, zd, tsend, xin, rt, p0, p1, hid,
    own, psend, precv, sbuf, r1, r2, fin, ret,
    yg_r, yd_r, zg_r, zd_r, tk_r, g_r, s_r, ret_r, snd,
):
    g, f, t = lax.axis_index("gr"), lax.axis_index("fs"), lax.axis_index("tp")
    z, y, x, c = f // NY, f % NY, t // 2, t % 2
    zz = g * NZ + z
    right, left = ((x + 1) % NX) * 2 + c, ((x + 3) % NX) * 2 + c
    opp, part = ((x + 2) % NX) * 2 + c, x * 2 + (1 - c)

    def send(src, dst, ssem, rsem, dev):
        pltpu.make_async_remote_copy(
            src_ref=src, dst_ref=dst, send_sem=ssem, recv_sem=rsem,
            device_id=dev, device_id_type=MESH,
        ).start()

    def arrived(dst, rsem):
        pltpu.make_async_remote_copy(
            src_ref=dst, dst_ref=dst, send_sem=snd.at[0], recv_sem=rsem,
            device_id=(g, f, part), device_id_type=MESH,
        ).wait_recv()

    def sent(ref, ssem):
        pltpu.make_async_remote_copy(
            src_ref=ref, dst_ref=ref, send_sem=ssem, recv_sem=yg_r.at[0],
            device_id=(g, f, part), device_id_type=MESH,
        ).wait_send()

    bar = pltpu.get_barrier_semaphore()

    def greet(dev):
        pl.semaphore_signal(bar, inc=1, device_id=dev, device_id_type=MESH)

    for tt in (part, right, left):
        greet((g, f, tt))
    loop(1, NF, lambda i: greet((g, (f + i) % NF, t)))
    loop(0, NZ, lambda i: greet((1 - g, i * NY + y, t)))

    gain[...] = jnp.broadcast_to(column(gain_t[...], 32), (32, 128))

    def cast(e):
        yy, z2 = e % NY, e // NY
        wg[yy, z2, 0:32, :] = (gain[...] * gate[e]).astype(BF)
        wg[yy, z2, 32:64, :] = (gain[...] * up[e]).astype(BF)
        wd[yy, z2] = down_t[e].astype(BF)

    loop(0, NF, cast)
    pl.semaphore_wait(bar, 3 + NF - 1 + NZ)

    def y_send(j, w, wy, ssem, rsems):
        yy = (y + ring_offset(j, NY)) % NY
        loop(0, NZ, lambda i: send(
            w.at[yy, i], wy.at[j - 1, i], ssem, rsems.at[j - 1], (g, z * NY + yy, t)))

    def z_send(jz, yy, block, s, wz, ssem, rsems):
        to = (zz + ring_offset(jz, NR)) % NR
        row = zz * NY + s
        send(block.at[to % NZ], wz.at[row], ssem, rsems.at[row],
             (to // NZ, (to % NZ) * NY + yy, t))

    loop(1, NY, lambda j: y_send(j, wg, wyg, snd.at[0], yg_r))
    loop(1, NR, lambda j: z_send(j, y, wg.at[y], y, zg, snd.at[1], zg_r))

    e_iota = lax.broadcasted_iota(jnp.int32, (NF, 256), 0)
    hit = (ids_t[0:1, :] == e_iota) | (ids_t[1:2, :] == e_iota)
    before = (
        lax.broadcasted_iota(jnp.int32, (256, 256), 0)
        < lax.broadcasted_iota(jnp.int32, (256, 256), 1)
    )
    rank = jnp.dot(hit.astype(F32).astype(BF), before.astype(F32).astype(BF),
                   preferred_element_type=F32)
    rt[...] = jnp.where(hit, rank, -1.0)
    r_iota = lax.broadcasted_iota(jnp.int32, (CAP, 256), 0).astype(F32)

    def slots(e):
        mask = rt[pl.ds(e, 1), :] == r_iota
        p0[e] = jnp.where(mask & (ids_t[0:1, :] == e), 1.0, 0.0).astype(BF)
        p1[e] = jnp.where(mask & (ids_t[1:2, :] == e), 1.0, 0.0).astype(BF)

    loop(0, NF, slots)
    floated = tok[...].astype(F32)
    inv = lax.rsqrt(jnp.mean(floated * floated, axis=-1, keepdims=True) + EPS)
    cols = pl.ds(pl.multiple_of(t * 256, 256), 256)
    normed = (tok[:, cols].astype(F32) * inv).astype(BF)

    def gather_rows(b):
        e = pl.ds(b * 8, 8)
        pick = (p0[e] + p1[e]).reshape(256, 256)
        rows = jnp.dot(pick, normed, preferred_element_type=F32)
        tsend[e] = rows.astype(BF).reshape(8, CAP, 256)

    loop(0, NZ, gather_rows)

    def t_send(i):
        e = ((z + i // NY) % NZ) * NY + (y + i % NY) % NY
        send(tsend.at[e], xin.at[t, f], snd.at[2], tk_r.at[f], (g, e, t))

    loop(1, NF, t_send)
    xin[t, f] = tsend[f]

    loop(1, NY, lambda j: y_send(j, wd, wyd, snd.at[8], yd_r))
    loop(1, NR, lambda j: z_send(j, y, wd.at[y], y, zd, snd.at[9], zd_r))
    zg[zz * NY + y] = wg[y, z]
    zd[zz * NY + y] = wd[y, z]

    def y_forward(j, wy, wz, ssem, rsems, yrsems):
        s = (y + NY - ring_offset(j, NY)) % NY
        arrived(wy.at[j - 1], yrsems.at[j - 1])
        loop(1, NR, lambda i: z_send(i, y, wy.at[j - 1], s, wz, ssem, rsems))
        wz[zz * NY + s] = wy[j - 1, z]

    loop(1, NY, lambda j: y_forward(j, wyg, zg, snd.at[1], zg_r, yg_r))

    def quarter(k):
        return (z + NZ - k) % NZ

    def pieces(tp, lo, n, kind, k, to):
        def one(i):
            blk = xin.at[tp, lo + i]
            send(blk, blk, snd.at[3], g_r.at[kind, k], (g, f, to))

        loop(0, n, one)

    def x_first(k):
        q = quarter(k)

        def one(i):
            s = q * NY + i

            @pl.when(s != f)
            def _():
                arrived(xin.at[t, s], tk_r.at[s])

            pieces(t, s, 1, 0, k, right)
            pieces(t, s, 1, 1, k, left)
            pieces(t, s, 1, 4, k, part)

        loop(0, NY, one)

    def x_second(k):
        q = quarter(k) * NY
        for side, kind, to, lo in ((left, 0, right, 0), (right, 1, left, 4)):
            arrived(xin.at[side, pl.ds(q, NY)], g_r.at[kind, k])
            pieces(side, q + lo, 4, kind + 2, k, to)
            pieces(side, q, NY, kind + 5, k, part)

    def x_third(k):
        q = quarter(k) * NY
        arrived(xin.at[opp, pl.ds(q, 4)], g_r.at[2, k])
        arrived(xin.at[opp, pl.ds(q + 4, 4)], g_r.at[3, k])
        pieces(opp, q, NY, 7, k, part)

    def x_step(k):
        @pl.when(k < NZ)
        def _():
            x_first(k)

        @pl.when((k >= 1) & (k < NZ + 1))
        def _():
            x_second(k - 1)

        @pl.when(k >= 2)
        def _():
            x_third(k - 2)

    loop(0, NZ + 2, x_step)
    loop(1, NY, lambda j: y_forward(j, wyd, zd, snd.at[9], zd_r, yd_r))
    flip = 1 - 2 * c

    def from_partner(k):
        q = pl.ds(quarter(k) * NY, NY)
        for side, kind in ((part, 4), (left + flip, 5), (right + flip, 6), (opp + flip, 7)):
            arrived(xin.at[side, q], g_r.at[kind, k])

    loop(0, NZ, from_partner)

    def w_arrived(i, wz, rsems):
        @pl.when(i // NY != zz)
        def _():
            arrived(wz.at[i], rsems.at[i])

    loop(0, 2 * NF, lambda i: w_arrived(i, zg, zg_r))

    def hidden(q):
        acc = jnp.zeros((256, 256), F32)
        for s in range(8):
            w = jnp.concatenate(
                [zg[8 * s:8 * s + 8, 0:32, :].reshape(256, 128),
                 zg[8 * s:8 * s + 8, 32:64, :].reshape(256, 128)], axis=1)
            acc += jnp.dot(xin[s, pl.ds(q * NY, NY)].reshape(256, 256), w,
                           preferred_element_type=F32)
        a, b = acc[:, 0:128], acc[:, 128:256]
        hid[pl.ds(2 * q, 2)] = (a / (1.0 + jnp.exp(-a)) * b).astype(BF).reshape(2, RB, 128)

    loop(0, NZ, hidden)
    loop(0, 2 * NF, lambda i: w_arrived(i, zd, zd_r))

    def which(k):
        return quarter(k // 2) * 2 + k % 2

    def layer(k):
        h = hid[which(k)]
        for j in range(NX):
            for cc in (1 - c, c):
                blk = ((x + j) % NX) * 2 + cc
                d = zd[pl.ds(blk * 8, 8)].reshape(256, 128)
                o = lax.dot_general(h, d, (((1,), (1,)), ((), ())), preferred_element_type=F32)
                if cc is c:
                    own[k, j] = o
                else:
                    psend[k, j] = o.astype(BF)
        send(psend.at[k], precv.at[k], snd.at[4], s_r.at[0, k], (g, f, part))

    LO, HI = pl.ds(0, RB // 2), pl.ds(RB // 2, RB // 2)

    def r_first(k):
        arrived(precv.at[k], s_r.at[0, k])
        sbuf[k, 1] = (own[k, 2] + precv[k, 2].astype(F32)).astype(BF)
        send(sbuf.at[k, 1, LO], r1.at[k, 0], snd.at[5], s_r.at[1, k], (g, f, right))
        send(sbuf.at[k, 1, HI], r1.at[k, 1], snd.at[5], s_r.at[2, k], (g, f, left))

    def r_second(k):
        for j, i, at, plain, to in ((1, 0, LO, HI, right), (3, 1, HI, LO, left)):
            arrived(r1.at[k, i], s_r.at[1 + i, k])
            sbuf[k, j - 1, at] = (
                own[k, j, at] + precv[k, j, at].astype(F32) + r1[k, i].astype(F32)
            ).astype(BF)
            sbuf[k, j - 1, plain] = (own[k, j, plain] + precv[k, j, plain].astype(F32)).astype(BF)
            send(sbuf.at[k, j - 1], r2.at[k, i], snd.at[6], s_r.at[3 + i, k], (g, f, to))

    def r_third(k):
        arrived(r2.at[k, 0], s_r.at[3, k])
        arrived(r2.at[k, 1], s_r.at[4, k])
        total = (own[k, 0] + precv[k, 0].astype(F32)) + r2[k, 0].astype(F32) + r2[k, 1].astype(F32)
        q = which(k)
        fin[q] = total.astype(BF).reshape(4, CAP, 256)

        def back(i):
            s = q * 4 + i

            @pl.when(s != f)
            def _():
                send(fin.at[q, i], ret.at[f], snd.at[7], ret_r.at[f], (g, s, t))

            @pl.when(s == f)
            def _():
                ret[s] = fin[q, i]

        loop(0, 4, back)

    def r_step(k):
        for lag, stage in ((0, layer), (1, r_first), (1 + LAG1, r_second), (1 + LAG1 + LAG2, r_third)):
            @pl.when((k >= lag) & (k < CH + lag))
            def _():
                stage(k - lag)

    loop(0, CH + 1 + LAG1 + LAG2, r_step)

    def store(i):
        gate_o[i] = zg[i, 0:32, :]
        up_o[i] = zg[i, 32:64, :]

    loop(0, 2 * NF, store)
    for j in range(16):
        blk = zd[4 * j:4 * j + 4].reshape(128, 128)
        down_o[:, 128 * j:128 * j + 128] = blk.astype(F32).T.astype(BF)
    s0, s1 = column(score_t[0:1, :], 256), column(score_t[1:2, :], 256)
    both = s0 + s1

    def back_arrived(i):
        @pl.when(i != f)
        def _():
            arrived(ret.at[i], ret_r.at[i])

    loop(0, NF, back_arrived)
    rows = ret[...].reshape(NF * CAP, 256)
    dims = (((0,), (0,)), ((), ()))
    a = lax.dot_general(p0[...].reshape(NF * CAP, 256), rows, dims, preferred_element_type=F32)
    b = lax.dot_general(p1[...].reshape(NF * CAP, 256), rows, dims, preferred_element_type=F32)
    mixed_o[...] = (a * (s0 / both) + b * (s1 / both)).astype(BF)

    nz = (NR - 1) * NY
    sent(wg.at[pl.ds(0, NY - 1)], snd.at[0])
    sent(zg.at[pl.ds(0, nz)], snd.at[1])
    sent(tsend.at[pl.ds(0, NF - 1)], snd.at[2])
    sent(xin.at[pl.ds(0, 7)], snd.at[3])
    sent(psend, snd.at[4])
    sent(r1, snd.at[5])
    sent(r2, snd.at[6])
    sent(ret.at[pl.ds(0, NF - 1)], snd.at[7])
    sent(wd.at[pl.ds(0, NY - 1)], snd.at[8])
    sent(zd.at[pl.ds(0, nz)], snd.at[9])


def write_out(gate_v, up_v, down_v, mixed_v, gate_o, up_o, down_o, mixed_o, sem):
    copies = [
        pltpu.make_async_copy(a, b, sem.at[i])
        for i, (a, b) in enumerate(
            ((gate_v, gate_o), (up_v, up_o), (down_v, down_o), (mixed_v, mixed_o)))
    ]
    for cp in copies:
        cp.start()
    for cp in copies:
        cp.wait()


def on_device(tokens, norm_gain, gate_train, up_train, down_train, expert_ids, route_score):
    vm = pl.BlockSpec(memory_space=pltpu.VMEM)
    hbm = pl.BlockSpec(memory_space=pl.ANY)
    dma = pltpu.SemaphoreType.DMA
    shapes = ((2 * NF, 32, 128), (2 * NF, 32, 128), (128, 2048), (256, 256))
    V = pltpu.VMEM
    held = pl.pallas_call(
        kernel,
        out_shape=tuple(V(s, BF) for s in shapes),
        in_specs=[vm] * 7,
        out_specs=(vm,) * 4,
        scratch_shapes=[
            V((32, 128), F32),
            V((NY, NZ, 64, 128), BF),
            V((NY, NZ, 32, 128), BF),
            V((NY - 1, NZ, 64, 128), BF),
            V((NY - 1, NZ, 32, 128), BF),
            V((2 * NF, 64, 128), BF),
            V((2 * NF, 32, 128), BF),
            V((NF, CAP, 256), BF),
            V((8, NF, CAP, 256), BF),
            V((NF, 256), F32),
            V((NF, CAP, 256), BF),
            V((NF, CAP, 256), BF),
            V((CH, RB, 128), BF),
            V((CH, NX, RB, 256), F32),
            V((CH, NX, RB, 256), BF),
            V((CH, NX, RB, 256), BF),
            V((CH, 3, RB, 256), BF),
            V((CH, 2, RB // 2, 256), BF),
            V((CH, 2, RB, 256), BF),
            V((CH, 4, CAP, 256), BF),
            V((NF, CAP, 256), BF),
            dma((NY - 1,)), dma((NY - 1,)), dma((2 * NF,)), dma((2 * NF,)), dma((NF,)),
            dma((8, NZ)), dma((5, CH)), dma((NF,)), dma((10,)),
        ],
        compiler_params=pltpu.CompilerParams(collective_id=0, has_side_effects=True),
    )(
        tokens, expert_ids.T, route_score.T, norm_gain[None, :], gate_train, up_train,
        down_train.transpose(0, 2, 1),
    )
    gate_r, up_r, down_r, mixed = pl.pallas_call(
        write_out,
        out_shape=tuple(jax.ShapeDtypeStruct(s, BF) for s in shapes),
        in_specs=[vm] * 4,
        out_specs=(hbm,) * 4,
        scratch_shapes=[dma((4,))],
    )(*[pltpu.with_memory_space_constraint(h, pltpu.VMEM) for h in held])
    return gate_r.reshape(1, 2048, 128), up_r.reshape(1, 2048, 128), down_r[None], mixed


def solution(mesh):
    return jax.shard_map(
        on_device,
        mesh=mesh,
        in_specs=(
            P(("gr", "fs"), None),
            P(("gr", "fs")),
            P(None, ("gr", "fs"), "tp"),
            P(None, ("gr", "fs"), "tp"),
            P(None, "tp", ("gr", "fs")),
            P(("gr", "fs"), None),
            P(("gr", "fs"), None),
        ),
        out_specs=(
            P("fs", None, "tp"),
            P("fs", None, "tp"),
            P("fs", "tp", None),
            P(("gr", "fs"), "tp"),
        ),
        check_vma=False,
    )
```

time: 111 us -> 98.7 us (0.89)
  local copies, waits for them, and re-layouts: 11.1 us -> 0 us
  Pallas kernels: 98.8 us -> 97.6 us
    unnamed x10 -> x0, local copies, waits for them, and re-layouts: 9.72 us -> none
    broadcast_in_dim x1 -> x0, local copies, waits for them, and re-layouts: 1.34 us -> none  [on_device(): norm_gain[:, None]]
    pallas_call x1 -> x2, Pallas kernels: 98.8 us -> 97.6 us  [the longest x1 96.4 us: on_device(): pl.pallas_call(kernel, out_shape=tuple((V(s, BF) for s in shapes)), in_sp...]
where the time goes in v2:
time: 98.7 us; the launch traced here: 98.2 us
  Pallas kernels  97.6 us (99%)
    pallas_call x1, Pallas kernels, on_device(): pl.pallas_call(kernel, out_shape=tuple((V(s, BF) for s in shapes)), in_sp...  96.4 us

profile of v2, /device:TPU:1, one launch (start us, length us, event | category | flops | bytes accessed | tf_op | source)
XLA Modules:
  0.0 98.2 jit_solution(9978799847777626949)
XLA Ops:
  0.6 96.4 %shard_map.102 = (bf16[64,32,128]{2,1,0:T(8,128)(2,1)S(1)}, bf16[64,32,128]{2,1,0:T(8,128)(2,1)S(1)}, bf16[128,2048]{1,0:T(8,128)(2,1)S(1)}, bf16[256,256]{1,0:T(8,128)(2,1)S(1)}) custom-call(bf16[256,2048]{1,0:T(8,128)(2,1)} %tok.1, s32[2,256]{1,0:T(2,128)} %bitcast.8, f32[2,256]{1,0:T(2,128)} %bitcast.9, f32[1,32]{1,0:T(1,128)} %bitcast.10, ...), custom_call_target="tpu_custom_call" | custom-call | tf_op jit(solution)/shard_map/pallas_call | solution.py:351
  97.0 1.2 %shard_map.103 = (bf16[64,32,128]{2,1,0:T(8,128)(2,1)}, bf16[64,32,128]{2,1,0:T(8,128)(2,1)}, bf16[128,2048]{1,0:T(8,128)(2,1)}, bf16[256,256]{1,0:T(8,128)(2,1)}) custom-call(bf16[64,32,128]{2,1,0:T(8,128)(2,1)S(1)} %get-tuple-element.12.gate_v, bf16[64,32,128]{2,1,0:T(8,128)(2,1)S(1)} %get-tuple-element.13.up_v, ...), custom_call_target="tpu_custom_call" | custom-call | tf_op jit(solution)/shard_map/pallas_call | solution.py:386

commit v3 on v2

--- a/solution.py
+++ b/solution.py
@@ -10,14 +10,22 @@
 NF = NY * NZ
 NR = 2 * NZ
 CAP = 32
-CH, RB = 8, 128
-LAG1, LAG2 = 2, 2
+CH = 8
+RB, CQ = 1024 // CH, CH // NZ
+LAG1, LAG2 = 3, 3
 MESH = pl.DeviceIdType.MESH
 BF, F32 = jnp.bfloat16, jnp.float32
 
 
-def ring_offset(j, n):
-    return jnp.where(j % 2 == 1, (j + 1) // 2, (n - j // 2) % n)
+OFFS = (1, 7, 2, 6, 3, 5, 4)
+
+
+def rem(a, n):
+    return lax.rem(a, jnp.int32(n))
+
+
+def div(a, n):
+    return lax.div(a, jnp.int32(n))
 
 
 def loop(lo, hi, fn):
@@ -34,17 +42,18 @@
 
 
 def kernel(
-    tok, ids_t, score_t, gain_t, gate, up, down_t,
+    tok_h, ids_t, score_t, gain_t, gate_h, up_h, down_h,
     gate_o, up_o, down_o, mixed_o,
-    gain, wg, wd, wyg, wyd, zg, zd, tsend, xin, rt, p0, p1, hid,
-    own, psend, precv, sbuf, r1, r2, fin, ret,
-    yg_r, yd_r, zg_r, zd_r, tk_r, g_r, s_r, ret_r, snd,
+    tok, gate, up, down_t, gain, wg, wd, wyg, wyd, zg, zd, tsend, xin, rt, p0, p1, hid,
+    own, psend, precv, sbuf, r1, r2, fin, ret, acc,
+    yg_r, yd_r, zg_r, zd_r, tk_r, g_r, s_r, ret_r, snd, in_sem, ready,
 ):
     g, f, t = lax.axis_index("gr"), lax.axis_index("fs"), lax.axis_index("tp")
-    z, y, x, c = f // NY, f % NY, t // 2, t % 2
+    z, y, x, c = div(f, NY), rem(f, NY), div(t, 2), rem(t, 2)
     zz = g * NZ + z
-    right, left = ((x + 1) % NX) * 2 + c, ((x + 3) % NX) * 2 + c
-    opp, part = ((x + 2) % NX) * 2 + c, x * 2 + (1 - c)
+    right, left = rem(x + 1, NX) * 2 + c, rem(x + 3, NX) * 2 + c
+    opp, part = rem(x + 2, NX) * 2 + c, x * 2 + (1 - c)
+    z_peer = [(div(q, NZ), rem(q, NZ)) for q in (rem(zz + o, NR) for o in OFFS)]
 
     def send(src, dst, ssem, rsem, dev):
         pltpu.make_async_remote_copy(
@@ -64,6 +73,13 @@
             device_id=(g, f, part), device_id_type=MESH,
         ).wait_send()
 
+    loads = [
+        pltpu.make_async_copy(a, b, in_sem.at[i])
+        for i, (a, b) in enumerate(((gate_h, gate), (up_h, up), (down_h, down_t), (tok_h, tok)))
+    ]
+    for cp in loads:
+        cp.start()
+
     bar = pltpu.get_barrier_semaphore()
 
     def greet(dev):
@@ -71,33 +87,44 @@
 
     for tt in (part, right, left):
         greet((g, f, tt))
-    loop(1, NF, lambda i: greet((g, (f + i) % NF, t)))
-    loop(0, NZ, lambda i: greet((1 - g, i * NY + y, t)))
+    for o in OFFS:
+        greet((g, z * NY + rem(y + o, NY), t))
+    for g2, z2 in z_peer:
+        greet((g2, z2 * NY + y, t))
 
     gain[...] = jnp.broadcast_to(column(gain_t[...], 32), (32, 128))
 
-    def cast(e):
-        yy, z2 = e % NY, e // NY
-        wg[yy, z2, 0:32, :] = (gain[...] * gate[e]).astype(BF)
-        wg[yy, z2, 32:64, :] = (gain[...] * up[e]).astype(BF)
-        wd[yy, z2] = down_t[e].astype(BF)
-
-    loop(0, NF, cast)
-    pl.semaphore_wait(bar, 3 + NF - 1 + NZ)
-
-    def y_send(j, w, wy, ssem, rsems):
-        yy = (y + ring_offset(j, NY)) % NY
-        loop(0, NZ, lambda i: send(
-            w.at[yy, i], wy.at[j - 1, i], ssem, rsems.at[j - 1], (g, z * NY + yy, t)))
-
-    def z_send(jz, yy, block, s, wz, ssem, rsems):
-        to = (zz + ring_offset(jz, NR)) % NR
+    def cast(yy):
+        for z2 in range(NZ):
+            e = z2 * NY + yy
+            wg[yy, z2, 0:32, :] = (gain[...] * gate[e]).astype(BF)
+            wg[yy, z2, 32:64, :] = (gain[...] * up[e]).astype(BF)
+
+    def cast_down(yy):
+        for z2 in range(NZ):
+            wd[yy, z2] = down_t[z2 * NY + yy].astype(BF)
+
+    loads[0].wait()
+    loads[1].wait()
+    loop(0, NY, cast)
+    pl.semaphore_wait(bar, 3 + NY - 1 + NR - 1)
+    loop(1, NZ, lambda i: pl.semaphore_signal(
+        ready, inc=1, device_id=(g, rem(z + i, NZ) * NY + y, t), device_id_type=MESH))
+
+    def y_sends(w, wy, ssem, rsems):
+        for j, o in enumerate(OFFS):
+            yy = rem(y + o, NY)
+            for i in range(NZ):
+                send(w.at[yy, i], wy.at[j, i], ssem, rsems.at[j], (g, z * NY + yy, t))
+
+    def z_sends(block, s, wz, ssem, rsems):
         row = zz * NY + s
-        send(block.at[to % NZ], wz.at[row], ssem, rsems.at[row],
-             (to // NZ, (to % NZ) * NY + yy, t))
-
-    loop(1, NY, lambda j: y_send(j, wg, wyg, snd.at[0], yg_r))
-    loop(1, NR, lambda j: z_send(j, y, wg.at[y], y, zg, snd.at[1], zg_r))
+        for g2, z2 in z_peer:
+            send(block.at[z2], wz.at[row], ssem, rsems.at[row], (g2, z2 * NY + y, t))
+        wz[row] = block[z]
+
+    y_sends(wg, wyg, snd.at[0], yg_r)
+    z_sends(wg.at[y], y, zg, snd.at[1], zg_r)
 
     e_iota = lax.broadcasted_iota(jnp.int32, (NF, 256), 0)
     hit = (ids_t[0:1, :] == e_iota) | (ids_t[1:2, :] == e_iota)
@@ -116,41 +143,46 @@
         p1[e] = jnp.where(mask & (ids_t[1:2, :] == e), 1.0, 0.0).astype(BF)
 
     loop(0, NF, slots)
+    loads[3].wait()
     floated = tok[...].astype(F32)
     inv = lax.rsqrt(jnp.mean(floated * floated, axis=-1, keepdims=True) + EPS)
     cols = pl.ds(pl.multiple_of(t * 256, 256), 256)
     normed = (tok[:, cols].astype(F32) * inv).astype(BF)
 
-    def gather_rows(b):
-        e = pl.ds(b * 8, 8)
+    def dispatch(k):
+        q = rem(z + k, NZ)
+        e = pl.ds(q * NY, NY)
         pick = (p0[e] + p1[e]).reshape(256, 256)
         rows = jnp.dot(pick, normed, preferred_element_type=F32)
         tsend[e] = rows.astype(BF).reshape(8, CAP, 256)
-
-    loop(0, NZ, gather_rows)
-
-    def t_send(i):
-        e = ((z + i // NY) % NZ) * NY + (y + i % NY) % NY
-        send(tsend.at[e], xin.at[t, f], snd.at[2], tk_r.at[f], (g, e, t))
-
-    loop(1, NF, t_send)
+        for i in range(NY):
+            to = q * NY + rem(y + i, NY)
+            if i:
+                send(tsend.at[to], xin.at[t, f], snd.at[2], tk_r.at[f], (g, to, t))
+            else:
+                @pl.when(to != f)
+                def _():
+                    send(tsend.at[to], xin.at[t, f], snd.at[2], tk_r.at[f], (g, to, t))
+
+    pl.semaphore_wait(ready, NZ - 1)
+    loop(0, NZ, dispatch)
     xin[t, f] = tsend[f]
 
-    loop(1, NY, lambda j: y_send(j, wd, wyd, snd.at[8], yd_r))
-    loop(1, NR, lambda j: z_send(j, y, wd.at[y], y, zd, snd.at[9], zd_r))
-    zg[zz * NY + y] = wg[y, z]
-    zd[zz * NY + y] = wd[y, z]
+    loads[2].wait()
+    loop(0, NY, cast_down)
+    y_sends(wd, wyd, snd.at[8], yd_r)
+    z_sends(wd.at[y], y, zd, snd.at[9], zd_r)
 
     def y_forward(j, wy, wz, ssem, rsems, yrsems):
-        s = (y + NY - ring_offset(j, NY)) % NY
-        arrived(wy.at[j - 1], yrsems.at[j - 1])
-        loop(1, NR, lambda i: z_send(i, y, wy.at[j - 1], s, wz, ssem, rsems))
-        wz[zz * NY + s] = wy[j - 1, z]
-
-    loop(1, NY, lambda j: y_forward(j, wyg, zg, snd.at[1], zg_r, yg_r))
+        s = rem(y + NY - OFFS[j], NY)
+        arrived(wy.at[j], yrsems.at[j])
+        z_sends(wy.at[j], s, wz, ssem, rsems)
+
+    for j in range(NY - 1):
+        y_forward(j, wyg, zg, snd.at[1], zg_r, yg_r)
 
     def quarter(k):
-        return (z + NZ - k) % NZ
+        return rem(z + NZ - k, NZ)
 
     def pieces(tp, lo, n, kind, k, to):
         def one(i):
@@ -202,7 +234,8 @@
             x_third(k - 2)
 
     loop(0, NZ + 2, x_step)
-    loop(1, NY, lambda j: y_forward(j, wyd, zd, snd.at[9], zd_r, yd_r))
+    for j in range(NY - 1):
+        y_forward(j, wyd, zd, snd.at[9], zd_r, yd_r)
     flip = 1 - 2 * c
 
     def from_partner(k):
@@ -213,7 +246,7 @@
     loop(0, NZ, from_partner)
 
     def w_arrived(i, wz, rsems):
-        @pl.when(i // NY != zz)
+        @pl.when(div(i, NY) != zz)
         def _():
             arrived(wz.at[i], rsems.at[i])
 
@@ -228,19 +261,19 @@
             acc += jnp.dot(xin[s, pl.ds(q * NY, NY)].reshape(256, 256), w,
                            preferred_element_type=F32)
         a, b = acc[:, 0:128], acc[:, 128:256]
-        hid[pl.ds(2 * q, 2)] = (a / (1.0 + jnp.exp(-a)) * b).astype(BF).reshape(2, RB, 128)
+        hid[pl.ds(CQ * q, CQ)] = (a / (1.0 + jnp.exp(-a)) * b).astype(BF).reshape(CQ, RB, 128)
 
     loop(0, NZ, hidden)
     loop(0, 2 * NF, lambda i: w_arrived(i, zd, zd_r))
 
     def which(k):
-        return quarter(k // 2) * 2 + k % 2
+        return rem(z + 1 + div(k, CQ), NZ) * CQ + rem(k, CQ)
 
     def layer(k):
         h = hid[which(k)]
         for j in range(NX):
             for cc in (1 - c, c):
-                blk = ((x + j) % NX) * 2 + cc
+                blk = rem(x + j, NX) * 2 + cc
                 d = zd[pl.ds(blk * 8, 8)].reshape(256, 128)
                 o = lax.dot_general(h, d, (((1,), (1,)), ((), ())), preferred_element_type=F32)
                 if cc is c:
@@ -271,10 +304,10 @@
         arrived(r2.at[k, 1], s_r.at[4, k])
         total = (own[k, 0] + precv[k, 0].astype(F32)) + r2[k, 0].astype(F32) + r2[k, 1].astype(F32)
         q = which(k)
-        fin[q] = total.astype(BF).reshape(4, CAP, 256)
+        fin[q] = total.astype(BF).reshape(NY // CQ, CAP, 256)
 
         def back(i):
-            s = q * 4 + i
+            s = q * (NY // CQ) + i
 
             @pl.when(s != f)
             def _():
@@ -284,7 +317,7 @@
             def _():
                 ret[s] = fin[q, i]
 
-        loop(0, 4, back)
+        loop(0, NY // CQ, back)
 
     def r_step(k):
         for lag, stage in ((0, layer), (1, r_first), (1 + LAG1, r_second), (1 + LAG1 + LAG2, r_third)):
@@ -305,17 +338,25 @@
     s0, s1 = column(score_t[0:1, :], 256), column(score_t[1:2, :], 256)
     both = s0 + s1
 
-    def back_arrived(i):
-        @pl.when(i != f)
-        def _():
-            arrived(ret.at[i], ret_r.at[i])
-
-    loop(0, NF, back_arrived)
-    rows = ret[...].reshape(NF * CAP, 256)
-    dims = (((0,), (0,)), ((), ()))
-    a = lax.dot_general(p0[...].reshape(NF * CAP, 256), rows, dims, preferred_element_type=F32)
-    b = lax.dot_general(p1[...].reshape(NF * CAP, 256), rows, dims, preferred_element_type=F32)
-    mixed_o[...] = (a * (s0 / both) + b * (s1 / both)).astype(BF)
+    acc[...] = jnp.zeros_like(acc)
+
+    def combine(k):
+        q = rem(z + NZ - 1 - k, NZ)
+
+        def back_arrived(i):
+            @pl.when(q * NY + i != f)
+            def _():
+                arrived(ret.at[q * NY + i], ret_r.at[q * NY + i])
+
+        loop(0, NY, back_arrived)
+        e = pl.ds(q * NY, NY)
+        rows = ret[e].reshape(256, 256)
+        for i, p in enumerate((p0, p1)):
+            acc[i] += lax.dot_general(p[e].reshape(256, 256), rows, (((0,), (0,)), ((), ())),
+                                      preferred_element_type=F32)
+
+    loop(0, NZ, combine)
+    mixed_o[...] = (acc[0] * (s0 / both) + acc[1] * (s1 / both)).astype(BF)
 
     nz = (NR - 1) * NY
     sent(wg.at[pl.ds(0, NY - 1)], snd.at[0])
@@ -351,9 +392,10 @@
     held = pl.pallas_call(
         kernel,
         out_shape=tuple(V(s, BF) for s in shapes),
-        in_specs=[vm] * 7,
+        in_specs=[hbm, vm, vm, vm, hbm, hbm, hbm],
         out_specs=(vm,) * 4,
         scratch_shapes=[
+            V((256, 2048), BF), V((NF, 32, 128), F32), V((NF, 32, 128), F32), V((NF, 32, 128), F32),
             V((32, 128), F32),
             V((NY, NZ, 64, 128), BF),
             V((NY, NZ, 32, 128), BF),
@@ -373,10 +415,12 @@
             V((CH, 3, RB, 256), BF),
             V((CH, 2, RB // 2, 256), BF),
             V((CH, 2, RB, 256), BF),
-            V((CH, 4, CAP, 256), BF),
+            V((CH, NY // CQ, CAP, 256), BF),
             V((NF, CAP, 256), BF),
+            V((2, 256, 256), F32),
             dma((NY - 1,)), dma((NY - 1,)), dma((2 * NF,)), dma((2 * NF,)), dma((NF,)),
-            dma((8, NZ)), dma((5, CH)), dma((NF,)), dma((10,)),
+            dma((8, NZ)), dma((5, CH)), dma((NF,)), dma((10,)), dma((4,)),
+            pltpu.SemaphoreType.REGULAR,
         ],
         compiler_params=pltpu.CompilerParams(collective_id=0, has_side_effects=True),
     )(

time: 98.7 us -> 94 us (0.952)
  Pallas kernels: 97.6 us -> 93 us
    pallas_call x1, Pallas kernels: 96.4 us -> 91.8 us  [on_device(): pl.pallas_call(kernel, out_shape=tuple((V(s, BF) for s in shapes)), in_sp...]
where the time goes in v3:
time: 94 us; the launch traced here: 93.6 us
  Pallas kernels  93 us (99%)
    pallas_call x1, Pallas kernels, on_device(): pl.pallas_call(kernel, out_shape=tuple((V(s, BF) for s in shapes)), in_sp...  91.8 us

profile of v3, /device:TPU:1, one launch (start us, length us, event | category | flops | bytes accessed | tf_op | source)
XLA Modules:
  0.0 93.6 jit_solution(14345138171190459817)
XLA Ops:
  0.6 91.8 %shard_map.102 = (bf16[64,32,128]{2,1,0:T(8,128)(2,1)S(1)}, bf16[64,32,128]{2,1,0:T(8,128)(2,1)S(1)}, bf16[128,2048]{1,0:T(8,128)(2,1)S(1)}, bf16[256,256]{1,0:T(8,128)(2,1)S(1)}) custom-call(bf16[256,2048]{1,0:T(8,128)(2,1)} %tok_h.1, s32[2,256]{1,0:T(2,128)} %bitcast.8, f32[2,256]{1,0:T(2,128)} %bitcast.9, f32[1,32]{1,0:T(1,128)} %bitcast.10, ...), custom_call_target="tpu_custom_call" | custom-call | tf_op jit(solution)/shard_map/pallas_call | solution.py:392
  92.4 1.2 %shard_map.103 = (bf16[64,32,128]{2,1,0:T(8,128)(2,1)}, bf16[64,32,128]{2,1,0:T(8,128)(2,1)}, bf16[128,2048]{1,0:T(8,128)(2,1)}, bf16[256,256]{1,0:T(8,128)(2,1)}) custom-call(bf16[64,32,128]{2,1,0:T(8,128)(2,1)S(1)} %get-tuple-element.12.gate_v, bf16[64,32,128]{2,1,0:T(8,128)(2,1)S(1)} %get-tuple-element.13.up_v, ...), custom_call_target="tpu_custom_call" | custom-call | tf_op jit(solution)/shard_map/pallas_call | solution.py:430

commit v4 on v3

--- a/solution.py
+++ b/solution.py
@@ -178,8 +178,6 @@
         arrived(wy.at[j], yrsems.at[j])
         z_sends(wy.at[j], s, wz, ssem, rsems)
 
-    for j in range(NY - 1):
-        y_forward(j, wyg, zg, snd.at[1], zg_r, yg_r)
 
     def quarter(k):
         return rem(z + NZ - k, NZ)
@@ -225,6 +223,11 @@
         def _():
             x_first(k)
 
+        @pl.when(k == 3)
+        def _():
+            for j in range(NY - 1):
+                y_forward(j, wyd, zd, snd.at[9], zd_r, yd_r)
+
         @pl.when((k >= 1) & (k < NZ + 1))
         def _():
             x_second(k - 1)
@@ -233,9 +236,12 @@
         def _():
             x_third(k - 2)
 
-    loop(0, NZ + 2, x_step)
-    for j in range(NY - 1):
-        y_forward(j, wyd, zd, snd.at[9], zd_r, yd_r)
+    for j in range(0, 4):
+        y_forward(j, wyg, zg, snd.at[1], zg_r, yg_r)
+    x_step(jnp.int32(0))
+    for j in range(4, 7):
+        y_forward(j, wyg, zg, snd.at[1], zg_r, yg_r)
+    loop(1, NZ + 2, x_step)
     flip = 1 - 2 * c
 
     def from_partner(k):

time: 94 us -> 93.1 us (level)
  no operation moved by 1% of the time
where the time goes in v4:
time: 93.1 us; the launch traced here: 92.9 us
  Pallas kernels  92.3 us (99%)
    pallas_call x1, Pallas kernels, on_device(): pl.pallas_call(kernel, out_shape=tuple((V(s, BF) for s in shapes)), in_sp...  91 us

profile of v4, /device:TPU:1, one launch (start us, length us, event | category | flops | bytes accessed | tf_op | source)
XLA Modules:
  0.0 92.9 jit_solution(8285571386908200247)
XLA Ops:
  0.6 91.0 %shard_map.102 = (bf16[64,32,128]{2,1,0:T(8,128)(2,1)S(1)}, bf16[64,32,128]{2,1,0:T(8,128)(2,1)S(1)}, bf16[128,2048]{1,0:T(8,128)(2,1)S(1)}, bf16[256,256]{1,0:T(8,128)(2,1)S(1)}) custom-call(bf16[256,2048]{1,0:T(8,128)(2,1)} %tok_h.1, s32[2,256]{1,0:T(2,128)} %bitcast.8, f32[2,256]{1,0:T(2,128)} %bitcast.9, f32[1,32]{1,0:T(1,128)} %bitcast.10, ...), custom_call_target="tpu_custom_call" | custom-call | tf_op jit(solution)/shard_map/pallas_call | solution.py:398
  91.7 1.2 %shard_map.103 = (bf16[64,32,128]{2,1,0:T(8,128)(2,1)}, bf16[64,32,128]{2,1,0:T(8,128)(2,1)}, bf16[128,2048]{1,0:T(8,128)(2,1)}, bf16[256,256]{1,0:T(8,128)(2,1)}) custom-call(bf16[64,32,128]{2,1,0:T(8,128)(2,1)S(1)} %get-tuple-element.12.gate_v, bf16[64,32,128]{2,1,0:T(8,128)(2,1)S(1)} %get-tuple-element.13.up_v, ...), custom_call_target="tpu_custom_call" | custom-call | tf_op jit(solution)/shard_map/pallas_call | solution.py:436
